TPU v7x, 512 devices: a whole 4x4x16 slice. The times are simulated.
512 devices in a mesh: rep: 2 (over z_hi), fs: 32 (over z_lo, y), tp: 8 (over x, core).
Axes of the slice: x: 4, y: 4, z: 16 (z_hi: 2, z_lo: 8; z = z_hi * 8 + z_lo), core: 2. Of those that a mesh axis runs over, the one named last changes fastest.
Arguments:
- tokens: bfloat16 [49152, 2048], P(('rep', 'fs', 'tp')), may hold values from -6 to 6
- norm_gain: float32 [2048], replicated, may hold values from 0.1 to 1.9
- gate_weight: float32 [2048, 5632], P('fs', 'tp'), may hold values from -0.125 to 0.125
- up_weight: float32 [2048, 5632], P('fs', 'tp'), may hold values from -0.125 to 0.125
- gate_scale: float32 [5632], P('tp'), may hold values from 0.3 to 3
- up_scale: float32 [5632], P('tp'), may hold values from 0.3 to 3
- down_weight: float32 [5632, 2048], P('tp', 'fs'), may hold values from -0.078125 to 0.078125
- down_scale: float32 [2048], replicated, may hold values from 0.3 to 3
Outputs:
- mixed: bfloat16 [49152, 2048], P(('rep', 'fs', 'tp'))
All inputs are finite; a program needn't handle non-finite values.
Results may differ from a plain program's by a relative error of at most 0.014.
Values may be sent and summed in bfloat16 or wider, within the bound.
A program may use at most 64 MiB of HBM per device.

v0:
```python
import jax
import jax.numpy as jnp
from jax import lax
from jax.sharding import PartitionSpec as P


def joined_along(blocks, dim):
    shape = list(blocks.shape[1:])
    shape[dim] *= blocks.shape[0]
    return jnp.moveaxis(blocks, 0, dim).reshape(shape)


def sent_to_all(shard, axis):
    size = lax.axis_size(axis)
    return lax.all_to_all(
        jnp.broadcast_to(shard[None], (size, *shard.shape)), axis, 0, 0, tiled=True
    )


def gather_directly(shard, axis, dim):
    return joined_along(sent_to_all(shard, axis), dim)


def in_one_piece(arrays, axis, dim, along):
    both = jnp.concatenate(arrays, axis=along)
    out, at, gathered = (lax.all_gather(both, axis, axis=dim, tiled=True), 0, [])
    for a in arrays:
        gathered.append(lax.slice_in_dim(out, at, at + a.shape[along], axis=along))
        at += a.shape[along]
    return tuple(gathered)


def cut_along(shard, dim, size):
    shape = shard.shape
    blocks = shard.reshape(*shape[:dim], size, shape[dim] // size, *shape[dim + 1 :])
    return jnp.moveaxis(blocks, dim, 0)


def sum_at_owner(shard, axis, dim):
    size = lax.axis_size(axis)
    blocks = lax.all_to_all(cut_along(shard, dim, size), axis, 0, 0, tiled=True)
    return jnp.sum(blocks.astype(jnp.float32), axis=0)


def on_device(
    tokens, norm_gain, gate_weight, up_weight, gate_scale, up_scale, down_weight, down_scale
):
    values = tokens.astype(jnp.float32)
    own_normed = (
        values * lax.rsqrt(jnp.mean(values * values, axis=-1, keepdims=True) + 1e-06) * norm_gain
    ).astype(jnp.bfloat16)
    normed = gather_directly(own_normed, "tp", 0)
    gate_local = gate_weight.astype(jnp.bfloat16)
    up_local = up_weight.astype(jnp.bfloat16)
    gate_whole, up_whole = in_one_piece((gate_local, up_local), "fs", 0, 1)
    gate_value = jnp.dot(normed, gate_whole, preferred_element_type=jnp.float32)
    up_value = jnp.dot(normed, up_whole, preferred_element_type=jnp.float32)
    hidden = (jax.nn.silu(gate_value * gate_scale) * (up_value * up_scale)).astype(jnp.bfloat16)
    partial_value = jnp.dot(
        hidden,
        lax.all_gather(down_weight.astype(jnp.bfloat16), "fs", axis=1, tiled=True),
        preferred_element_type=jnp.float32,
    )
    partial_value = partial_value.astype(jnp.bfloat16).astype(jnp.float32)
    summed = sum_at_owner(partial_value.astype(jnp.bfloat16), "tp", 0)
    return (summed * down_scale).astype(jnp.bfloat16)


def solution(mesh):
    placed = (
        P(("rep", "fs", "tp"), None),
        P(),
        P("fs", "tp"),
        P("fs", "tp"),
        P("tp"),
        P("tp"),
        P("tp", "fs"),
        P(),
    )
    return jax.shard_map(
        on_device,
        mesh=mesh,
        in_specs=placed,
        out_specs=P(("rep", "fs", "tp"), None),
        check_vma=False,
    )
```

profile of v0, /device:TPU:1, one launch (start us, length us, event | category | flops | bytes accessed | tf_op | source)
XLA Modules:
  0.0 533.2 jit_solution(5803203277212147337)
XLA Ops:
  6.5 0.0 all-gather.3.cloned.1.call-start
  6.5 0.9 convert_element_type.31
  7.5 0.9 convert_element_type.32
  8.4 0.8 pad_maximum_fusion
  9.2 0.0 all-gather.3.cloned.1.call-update
  9.2 0.0 all-gather.5.cloned.1.call-start
  9.3 1.6 convert_element_type.34
  10.8 0.0 all-gather.5.cloned.1.call-update
  10.9 1.2 fusion.11
  12.1 1.2 fusion.13
  13.2 0.4 broadcast_in_dim.2
  13.6 47.1 %all_to_all.10 = bf16[8,96,2048]{2,1,0:T(8,128)(2,1)S(1)} all-to-all(bf16[8,96,2048]{2,1,0:T(8,128)(2,1)S(1)} %broadcast_in_dim.2), channel_id=1, replica_groups=mesh['rep'=2,'fs'=32,'tp'=8] {'tp'}, dimensions={0} | all-to-all | bytes 6291456 | tf_op jit(solution)/shard_map/all_to_all | solution.py:15
  60.7 165.4 %all-gather.3.cloned.1.call-done = bf16[2048,1408]{1,0:T(8,128)(2,1)} async-done(((bf16[64,1408]{1,0:T(8,128)(2,1)}), bf16[2048,1408]{1,0:T(8,128)(2,1)}) %all-gather.3.cloned.1.call-update) | async-done | bytes 5767184 | tf_op jit(solution)/shard_map/all_gather | solution.py:26
  226.1 0.0 copy-start.1
  226.1 0.0 copy-start.2
  226.1 6.8 %fusion = f32[768,704]{0,1:T(8,128)} fusion(bf16[768,2048]{1,0:T(8,128)(2,1)S(1)} %bitcast.5, bf16[2048,1408]{1,0:T(8,128)(2,1)} %all-gather.3.cloned.1.call-done), kind=kOutput, calls=%fused_computation.2 | convolution fusion | flops 2214592512 | bytes 8454144 | tf_op jit(solution)/shard_map/dot_general | solution.py:57
  232.8 215.9 %all-gather.5.cloned.1.call-done = bf16[704,2048]{0,1:T(8,128)(2,1)} async-done(((bf16[704,64]{0,1:T(8,128)(2,1)}), bf16[704,2048]{0,1:T(8,128)(2,1)}) %all-gather.5.cloned.1.call-update) | async-done | bytes 2883600 | tf_op jit(solution)/shard_map/all_gather | solution.py:61
  448.7 0.0 copy-done.1
  448.7 0.0 copy-done.2
  448.7 11.7 %convolution_convert_fusion = bf16[768,2048]{1,0:T(8,128)(2,1)} fusion(bf16[704,2048]{0,1:T(8,128)(2,1)} %all-gather.5.cloned.1.call-done, f32[768,704]{0,1:T(8,128)} %fusion, bf16[768,2048]{1,0:T(8,128)(2,1)S(1)} %bitcast.6, bf16[2048,1408]{1,0:T(8,128)(2,1)} %all-gather.3.cloned.1.call-done, f32[704]{0:T(1024)S(1)} %copy-done.1, f32[704]{0:T(1024)S(1)} %copy-done.2), kind=kOutput, calls=%fused_computation.1 | convolution fusion | flops 4435083264 | bytes 14751232 | tf_op jit(solution)/shard_map/dot_general | solution.py:59
  460.4 64.4 %all_to_all.11 = bf16[8,96,2048]{2,1,0:T(8,128)(2,1)S(1)} all-to-all(bf16[8,96,2048]{2,1,0:T(8,128)(2,1)} %bitcast.7), channel_id=1, replica_groups=mesh['rep'=2,'fs'=32,'tp'=8] {'tp'}, dimensions={0} | all-to-all | bytes 6291456 | tf_op jit(solution)/shard_map/all_to_all | solution.py:41
  524.9 0.6 convert_reduce_fusion
  525.4 0.1 copy-done
  525.6 0.8 multiply_convert_fusion.1
  (2 shorter events, 0.0 us)
Async XLA Ops:
  6.5 219.5 %all-gather.3.cloned.1.call-start = ((), (), s32[]{:S(2)}) async-start(), calls=%async_computation.2 | async-start | bytes 5947392 | tf_op jit(solution)/shard_map/all_gather | solution.py:26
  9.2 439.5 %all-gather.5.cloned.1.call-start = ((), (), s32[]{:S(2)}) async-start(), calls=%async_computation.3 | async-start | bytes 3244032 | tf_op jit(solution)/shard_map/all_gather | solution.py:61
  226.1 222.6 %copy-start.1 = (f32[704]{0:T(1024)S(1)}, f32[704]{0:T(1024)}, u32[]{:S(2)}) copy-start(f32[704]{0:T(1024)} %param.13) | copy-start | bytes 8452
  226.1 222.6 %copy-start.2 = (f32[704]{0:T(1024)S(1)}, f32[704]{0:T(1024)}, u32[]{:S(2)}) copy-start(f32[704]{0:T(1024)} %param.12) | copy-start | bytes 8452
  524.9 0.7 copy-start
Sparse Core Ops, SparseCore 0:
  9.4 216.6 all-gather.2
  228.2 220.5 all-gather.4
where the time goes:
time: 534 us; the launch traced here: 533 us
  waiting for transfers between devices  381 us (71%)
  blocking collectives  112 us (21%)
  matrix products  18.5 us (3%)
  between operations  13.4 us (3%)
  other arithmetic  7.93 us (1%)
    all_gather x1, waiting for transfers between devices, on_device(): lax.all_gather(down_weight.astype(jnp.bfloat16), 'fs', axis=1, tiled=True)  216 us
    all_gather x1, waiting for transfers between devices, in_one_piece(): lax.all_gather(both, axis, axis=dim, tiled=True)  165 us
    all_to_all x1, blocking collectives, sum_at_owner(): blocks = lax.all_to_all(cut_along(shard, dim, size), axis, 0, 0, tiled=True)  64.4 us
    all_to_all x1, blocking collectives, sent_to_all(): lax.all_to_all(jnp.broadcast_to(shard[None], (size, *shard.shape)), axis,...  47.1 us
    dot_general x1, matrix products, on_device(): jnp.dot(hidden, lax.all_gather(down_weight.astype(jnp.bfloat16), 'fs', ax...  11.7 us
  transfers between devices with their start and end apart: 2, of which 2 were waited for; matrix products, arithmetic and copies ran while one was open for 2% of the time, Pallas kernels for 0%

commit v1 on v0

--- a/solution.py
+++ b/solution.py
@@ -2,6 +2,13 @@
 import jax.numpy as jnp
 from jax import lax
 from jax.sharding import PartitionSpec as P
+
+
+def swapped_in(block, axis, dim):
+    size = lax.axis_size(axis)
+    parts = jnp.stack([block for _ in range(size)])
+    parts = lax.all_to_all(parts, axis, split_axis=0, concat_axis=0)
+    return jnp.concatenate(parts, axis=dim)
 
 
 def joined_along(blocks, dim):
@@ -58,7 +65,7 @@
     hidden = (jax.nn.silu(gate_value * gate_scale) * (up_value * up_scale)).astype(jnp.bfloat16)
     partial_value = jnp.dot(
         hidden,
-        lax.all_gather(down_weight.astype(jnp.bfloat16), "fs", axis=1, tiled=True),
+        swapped_in(down_weight.astype(jnp.bfloat16), "fs", 1),
         preferred_element_type=jnp.float32,
     )
     partial_value = partial_value.astype(jnp.bfloat16).astype(jnp.float32)

time: 534 us -> 344 us (0.64)
  the two profiles are of different devices: /device:TPU:1 before, /device:TPU:120 now
where the time goes in v1:
time: 344 us
  waiting for transfers between devices  241 us (70%)
  blocking collectives  42 us (12%)
  starting transfers between devices  18.7 us (5%)
  matrix products  18.5 us (5%)
  between operations  13.5 us (4%)
  other arithmetic  5.43 us (2%)
  local copies, waits for them, and re-layouts  4.26 us (1%)
    all_gather x1, waiting for transfers between devices, in_one_piece(): lax.all_gather(both, axis, axis=dim, tiled=True)  205 us
    all_to_all x1, blocking collectives, sum_at_owner(): blocks = lax.all_to_all(cut_along(shard, dim, size), axis, 0, 0, tiled=True)  42 us
    all_to_all x1, waiting for transfers between devices, sent_to_all(): lax.all_to_all(jnp.broadcast_to(shard[None], (size, *shard.shape)), axis,...  36.6 us
    all_to_all x1, starting transfers between devices, swapped_in(): parts = lax.all_to_all(parts, axis, split_axis=0, concat_axis=0)  14.2 us
    dot_general x1, matrix products, on_device(): jnp.dot(hidden, swapped_in(down_weight.astype(jnp.bfloat16), 'fs', 1), pr...  11.7 us
  transfers between devices with their start and end apart: 3, of which 2 were waited for; matrix products, arithmetic and copies ran while one was open for 3% of the time, Pallas kernels for 0%

profile of v1, /device:TPU:120, one launch (start us, length us, event | category | flops | bytes accessed | tf_op | source)
XLA Modules:
  0.0 343.8 jit_solution(4646088823671281280)
XLA Ops:
  6.5 1.2 fusion.11
  7.7 1.2 fusion.13
  8.9 2.1 broadcast_in_dim.2
  11.0 0.0 copy-start
  11.0 4.4 %all-to-all-start = ((bf16[8,96,2048]{2,1,0:T(8,128)(2,1)}), bf16[8,96,2048]{2,1,0:T(8,128)(2,1)S(1)}, u32[]{:S(2)}, u32[]{:S(2)}) async-start(bf16[8,96,2048]{2,1,0:T(8,128)(2,1)} %broadcast_in_dim.2), calls=%async_computation | async-start | bytes 6291456 | tf_op jit(solution)/shard_map/all_to_all | solution.py:22
  15.4 0.0 all-gather.2.cloned.1.call-start
  15.5 0.0 copy-done
  15.5 0.0 copy-done.1
  15.5 0.8 pad_maximum_fusion
  16.3 0.0 all-gather.2.cloned.1.call-update
  16.3 0.9 convert_element_type.34
  17.3 36.6 %all-to-all-done = bf16[8,96,2048]{2,1,0:T(8,128)(2,1)S(1)} async-done(((bf16[8,96,2048]{2,1,0:T(8,128)(2,1)}), bf16[8,96,2048]{2,1,0:T(8,128)(2,1)S(1)}, u32[]{:S(2)}, u32[]{:S(2)}) %all-to-all-start) | async-done | bytes 3145760 | tf_op jit(solution)/shard_map/all_to_all | solution.py:22
  53.8 2.0 stack.2
  55.8 14.2 %all-to-all-start.1 = ((bf16[32,704,64]{1,2,0:T(8,128)(2,1)}), bf16[32,704,64]{1,2,0:T(8,128)(2,1)}, u32[]{:S(2)}, u32[]{:S(2)}) async-start(bf16[32,704,64]{1,2,0:T(8,128)(2,1)} %stack.2), calls=%async_computation.1 | async-start | bytes 6291456 | tf_op jit(solution)/shard_map/all_to_all | solution.py:10
  70.1 204.9 %all-gather.2.cloned.1.call-done = bf16[2048,1408]{1,0:T(8,128)(2,1)} async-done(((bf16[64,1408]{1,0:T(8,128)(2,1)}), bf16[2048,1408]{1,0:T(8,128)(2,1)}) %all-gather.2.cloned.1.call-update) | async-done | bytes 5767184 | tf_op jit(solution)/shard_map/all_gather | solution.py:33
  275.0 6.7 %fusion = f32[768,704]{0,1:T(8,128)} fusion(bf16[768,2048]{1,0:T(8,128)(2,1)S(1)} %bitcast.8, bf16[2048,1408]{1,0:T(8,128)(2,1)} %all-gather.2.cloned.1.call-done), kind=kOutput, calls=%fused_computation.2 | convolution fusion | flops 2214592512 | bytes 8454144 | tf_op jit(solution)/shard_map/dot_general | solution.py:64
  281.7 0.0 all-to-all-done.1
  281.7 0.0 copy-done.3
  281.7 0.0 copy-done.4
  281.7 11.7 %convolution_convert_fusion = bf16[768,2048]{1,0:T(8,128)(2,1)} fusion(bf16[704,2048]{0,1:T(8,128)(2,1)} %bitcast.2, f32[768,704]{0,1:T(8,128)} %fusion, bf16[768,2048]{1,0:T(8,128)(2,1)S(1)} %bitcast.9, bf16[2048,1408]{1,0:T(8,128)(2,1)} %all-gather.2.cloned.1.call-done, f32[704]{0:T(1024)S(1)} %copy-done.3, f32[704]{0:T(1024)S(1)} %copy-done.4), kind=kOutput, calls=%fused_computation.1 | convolution fusion | flops 4435083264 | bytes 14751232 | tf_op jit(solution)/shard_map/dot_general | solution.py:66
  293.5 42.0 %all_to_all.15 = bf16[8,96,2048]{2,1,0:T(8,128)(2,1)S(1)} all-to-all(bf16[8,96,2048]{2,1,0:T(8,128)(2,1)} %bitcast.10), channel_id=1, replica_groups=mesh['rep'=2,'fs'=32,'tp'=8] {'tp'}, dimensions={0} | all-to-all | bytes 6291456 | tf_op jit(solution)/shard_map/all_to_all | solution.py:48
  335.5 0.5 convert_reduce_fusion
  336.0 0.1 copy-done.2
  336.2 0.8 multiply_convert_fusion.1
  (7 shorter events, 0.0 us)
Async XLA Ops:
  11.0 4.5 %copy-start = (f32[64,704]{1,0:T(8,128)S(1)}, f32[64,704]{1,0:T(8,128)}, u32[]{:S(2)}) copy-start(f32[64,704]{1,0:T(8,128)} %param.11) | copy-start | bytes 540676
  11.0 4.5 %copy-start.1 = (f32[64,704]{1,0:T(8,128)S(1)}, f32[64,704]{1,0:T(8,128)}, u32[]{:S(2)}) copy-start(f32[64,704]{1,0:T(8,128)} %param.10) | copy-start | bytes 540676
  11.0 42.8 %all-to-all-start = ((bf16[8,96,2048]{2,1,0:T(8,128)(2,1)}), bf16[8,96,2048]{2,1,0:T(8,128)(2,1)S(1)}, u32[]{:S(2)}, u32[]{:S(2)}) async-start(bf16[8,96,2048]{2,1,0:T(8,128)(2,1)} %broadcast_in_dim.2), calls=%async_computation | async-start | bytes 6291456 | tf_op jit(solution)/shard_map/all_to_all | solution.py:22
  15.4 259.5 %all-gather.2.cloned.1.call-start = ((), (), s32[]{:S(2)}) async-start(), calls=%async_computation.3 | async-start | bytes 5947392 | tf_op jit(solution)/shard_map/all_gather | solution.py:33
  55.8 225.9 %all-to-all-start.1 = ((bf16[32,704,64]{1,2,0:T(8,128)(2,1)}), bf16[32,704,64]{1,2,0:T(8,128)(2,1)}, u32[]{:S(2)}, u32[]{:S(2)}) async-start(bf16[32,704,64]{1,2,0:T(8,128)(2,1)} %stack.2), calls=%async_computation.1 | async-start | bytes 6291456 | tf_op jit(solution)/shard_map/all_to_all | solution.py:10
  275.0 6.8 %copy-start.3 = (f32[704]{0:T(1024)S(1)}, f32[704]{0:T(1024)}, u32[]{:S(2)}) copy-start(f32[704]{0:T(1024)} %param.13) | copy-start | bytes 8452
  275.0 6.8 %copy-start.4 = (f32[704]{0:T(1024)S(1)}, f32[704]{0:T(1024)}, u32[]{:S(2)}) copy-start(f32[704]{0:T(1024)} %param.12) | copy-start | bytes 8452
  335.5 0.7 copy-start.2
Sparse Core Ops, SparseCore 0:
  18.3 256.6 all-gather.1
